TPU v7x, 32 devices: a whole 2x2x4 slice. The times are simulated.
32 devices in a mesh: sp: 16 (over z, y, x), tp: 2 (over core).
Axes of the slice: x: 2, y: 2, z: 4, core: 2. Of those that a mesh axis runs over, the one named last changes fastest.
Arguments:
- residual: bfloat16 [4096, 2048], P(('sp', 'tp')), may hold values from -6 to 6
- projected: bfloat16 [4096, 2048], P('sp', 'tp'), may hold values from -6 to 6
- group_weight: bfloat16 [4, 512, 512], P('tp'), may hold values from -0.25 to 0.25
- channel_scale: float32 [2048], P('tp'), may hold values from 0.1 to 1.9
- out_weight: bfloat16 [2048, 2048], replicated, may hold values from -0.125 to 0.125
- post_mix_gain: float32 [2048], replicated, may hold values from 0.1 to 1.9
- pre_ffn_gain: float32 [2048], replicated, may hold values from 0.1 to 1.9
- post_ffn_gain: float32 [2048], replicated, may hold values from 0.1 to 1.9
- route_ids: int32 [4096, 2], P(('sp', 'tp')), may hold values from 0 to 7, all different within a row; in each aligned block of 128 rows (0 to 127, 128 to 255, ...) at most 64 rows name the same one
- route_weight: float32 [4096, 2], P(('sp', 'tp')), may hold values from 0.1 to 1
- expert_gate: bfloat16 [16, 2048, 1792], P('sp', None, 'tp'), may hold values from -0.125 to 0.125
- expert_up: bfloat16 [16, 2048, 1792], P('sp', None, 'tp'), may hold values from -0.125 to 0.125
- expert_down: bfloat16 [16, 1792, 2048], P('sp', 'tp'), may hold values from -0.09375 to 0.09375
Outputs:
- layer_out: bfloat16 [4096, 2048], P(('sp', 'tp'))
Inputs may be any that keep to these rules, and one draw needn't show every extreme that they name: `route_ids`: each row names 2 different experts. In every aligned block of 128 rows (the rows of one device) no expert is named more than 64 times, a bound that some blocks reach.
All inputs are finite; a program needn't handle non-finite values.
Results may differ from a plain program's by a relative error of at most 0.014.
Values may be sent and summed in bfloat16 or wider, within the bound.
No kernel may reach another device: no remote copies, remote signals or barrier semaphores. Data moves between devices by JAX's collectives and lax.ppermute only.
A program may use at most 192 MiB of HBM per device.

v0:
```python
import jax
import jax.numpy as jnp
from jax import lax
from jax.sharding import PartitionSpec as P

GROUPS = 4
TOP = 2


EPS = 1e-06


def shifted(block, axis, distance):
    devices = range(lax.axis_size(axis))
    route = [(i - distance, i) for i in devices if i - distance in devices]
    return lax.ppermute(block, axis, route)


def rms_scale(values, gain):
    values = values.astype(jnp.float32)
    inverse = lax.rsqrt(jnp.mean(values * values, axis=-1, keepdims=True) + EPS)
    return values * inverse * gain


def window_sums(extended, lookback, count):
    levels = []
    current = extended
    window_span = 1
    for level_id in range(GROUPS):
        current = current[window_span:] + current[:-window_span]
        window_span = window_span * 2
        first = lookback - window_span + 1
        levels.append(lax.slice_in_dim(current, first, first + count, axis=0))
    return levels


def expert_whole_half(token_rows, gate_full, up_full, down_full, parts):
    flat_rows = token_rows.reshape(-1, token_rows.shape[-1])
    quarter = gate_full.shape[1] // parts
    total = jnp.zeros(flat_rows.shape, jnp.float32)
    for part_id in range(parts):
        low = part_id * quarter
        gate_value = jnp.dot(
            flat_rows, gate_full[:, low : low + quarter], preferred_element_type=jnp.float32
        )
        up_value = jnp.dot(
            flat_rows, up_full[:, low : low + quarter], preferred_element_type=jnp.float32
        )
        active = (jax.nn.silu(gate_value) * up_value).astype(jnp.bfloat16)
        term = jnp.dot(
            active, down_full[low : low + quarter], preferred_element_type=jnp.float32
        ).astype(jnp.bfloat16)
        total = total + term.astype(jnp.float32)
    return total.astype(jnp.bfloat16).reshape(token_rows.shape)


def body(
    residual,
    projected,
    group_weight,
    channel_scale,
    out_weight,
    post_mix_gain,
    pre_ffn_gain,
    post_ffn_gain,
    route_ids,
    route_weight,
    expert_gate,
    expert_up,
    expert_down,
):
    lookback = 2**GROUPS
    tokens_here = projected.shape[0]
    width_here = projected.shape[1]
    model_width = out_weight.shape[1]
    tp_count = lax.axis_size("tp")
    tp_index = lax.axis_index("tp")
    groups_here = GROUPS // tp_count
    group_width = width_here // groups_here
    earlier = shifted(projected[tokens_here - lookback :], "sp", 1)
    extended = jnp.concatenate([earlier, projected], 0).astype(jnp.float32)
    levels = window_sums(extended, lookback, tokens_here)
    offset = lax.axis_index("sp") * tokens_here
    position = (offset + lax.iota(jnp.int32, tokens_here) + 1).astype(jnp.float32)[:, None]
    pieces = []
    for local_group in range(groups_here):
        group_id = tp_index * groups_here + local_group
        low = local_group * group_width
        summed = jnp.zeros((tokens_here, group_width), jnp.float32)
        window_span = jnp.float32(1.0)
        for level_id in range(GROUPS):
            summed = jnp.where(
                group_id == level_id, levels[level_id][:, low : low + group_width], summed
            )
            window_span = jnp.where(
                group_id == level_id, jnp.float32(2.0 ** (level_id + 1)), window_span
            )
        own_part = projected[:, low : low + group_width].astype(jnp.float32)
        pieces.append(summed / jnp.minimum(position, window_span) - own_part)
    pooled = jnp.concatenate(pieces, 1).astype(jnp.bfloat16)
    grouped = jnp.einsum(
        "tgc,gce->tge",
        pooled.reshape(tokens_here, groups_here, group_width),
        group_weight,
        preferred_element_type=jnp.float32,
    )
    scaled = (grouped.reshape(tokens_here, width_here) * channel_scale).astype(jnp.bfloat16)
    weight_rows = lax.dynamic_slice_in_dim(out_weight, tp_index * width_here, width_here, 0)
    projection = lax.psum_scatter(
        jnp.dot(scaled, weight_rows, preferred_element_type=jnp.float32),
        "tp",
        scatter_dimension=0,
        tiled=True,
    )
    mixed = projection.astype(jnp.bfloat16)
    middle = (residual.astype(jnp.float32) + rms_scale(mixed, post_mix_gain)).astype(jnp.bfloat16)
    normed = rms_scale(middle, pre_ffn_gain).astype(jnp.bfloat16)
    row_count = normed.shape[0]
    experts_all = lax.axis_size("sp") // 2
    capacity = 2 * TOP * row_count // experts_all
    flat_ids = route_ids.reshape(-1)
    onehot = (flat_ids[:, None] == lax.iota(jnp.int32, experts_all)[None, :]).astype(jnp.int32)
    before = jnp.cumsum(onehot, 0) - onehot
    slot_ids = jnp.sum(before * onehot, 1)
    target = flat_ids * capacity + slot_ids
    source_row = lax.iota(jnp.int32, row_count * TOP) // TOP + 1
    source = jnp.zeros((experts_all * capacity,), jnp.int32).at[target].set(source_row)
    filled = source > 0
    table = jnp.where(
        filled[:, None], normed[jnp.maximum(source - 1, 0)], jnp.zeros((), jnp.bfloat16)
    )
    gate_part = expert_gate[0]
    up_part = expert_up[0]
    down_part = expert_down[0]
    gate_full, up_full = (
        lax.all_gather(gate_part, "tp", axis=1, tiled=True),
        lax.all_gather(up_part, "tp", axis=1, tiled=True),
    )
    down_full = lax.all_gather(down_part, "tp", axis=0, tiled=True)
    send_rows = jnp.repeat(table.reshape(experts_all, capacity, model_width), 2, axis=0)
    summed_half = expert_whole_half(
        lax.all_to_all(send_rows, "sp", split_axis=0, concat_axis=0, tiled=True),
        gate_full,
        up_full,
        down_full,
        tp_count,
    )
    returned = lax.all_to_all(summed_half, "sp", split_axis=0, concat_axis=0, tiled=True)
    pairs = returned.astype(jnp.float32).reshape(experts_all, 2, capacity, model_width)
    results = lax.optimization_barrier((pairs[:, 0] + pairs[:, 1]).astype(jnp.bfloat16))
    picked = results.reshape(experts_all * capacity, model_width)[target].astype(jnp.float32)
    weighted = picked * route_weight.reshape(-1)[:, None]
    ffn_sum = jnp.sum(weighted.reshape(row_count, TOP, model_width), 1)
    return (middle.astype(jnp.float32) + rms_scale(ffn_sum, post_ffn_gain)).astype(jnp.bfloat16)


def solution(mesh):
    in_specs = (
        P(("sp", "tp"), None),
        P("sp", "tp"),
        P("tp", None, None),
        P("tp"),
        P(),
        P(),
        P(),
        P(),
        P(("sp", "tp"), None),
        P(("sp", "tp"), None),
        P("sp", None, "tp"),
        P("sp", None, "tp"),
        P("sp", "tp", None),
    )
    out_specs = P(("sp", "tp"), None)
    return jax.shard_map(body, mesh=mesh, in_specs=in_specs, out_specs=out_specs, check_vma=False)
```

profile of v0, /device:TPU:14, one launch (start us, length us, event | category | flops | bytes accessed | tf_op | source)
XLA Modules:
  0.0 312.1 jit_solution(183979507235238384)
XLA Ops:
  6.5 0.8 slice.99
  7.4 3.4 %collective-permute-start = (bf16[16,1024]{1,0:T(8,128)(2,1)S(1)}, bf16[16,1024]{1,0:T(8,128)(2,1)S(1)}, u32[]{:S(2)}, u32[]{:S(2)}) collective-permute-start(bf16[16,1024]{1,0:T(8,128)(2,1)S(1)} %slice.99), channel_id=1, source_target_pairs={{0,2},{2,4},{4,6},{6,8},{8,10},{10,12},{12,14},{14,16},{16,18},{18... | collective-permute-start | bytes 98312 | tf_op jit(solution)/shard_map/ppermute | solution.py:16
  10.9 2.3 collective-permute-done
  13.2 1.2 maximum_convert_fusion
  14.4 0.2 slice_add_fusion.2
  14.5 0.2 slice_add_fusion.1
  14.8 0.2 slice_add_fusion
  15.1 0.7 copy-done.4
  15.8 0.3 fusion.42
  16.1 0.3 fusion.43
  16.4 0.4 convolution_bitcast_fusion
  16.8 0.3 copy.17
  17.2 0.2 fusion.26
  17.4 4.9 %fusion.2 = f32[256,2048]{1,0:T(8,128)} fusion(bf16[256,1024]{0,1:T(8,128)(2,1)S(1)} %fusion.26, bf16[2048,2048]{1,0:T(8,128)(2,1)} %param.17, s32[]{:T(128)S(6)} %select_n.124), kind=kOutput, calls=%fused_computation.8 | convolution fusion | flops 1073741824 | bytes 6815748 | tf_op jit(solution)/shard_map/dot_general | solution.py:110
  22.4 0.7 all-gather.9.cloned.1.call-update
  23.1 0.7 all-gather.7.cloned.1.call-update
  24.1 0.1 eq.65
  24.3 0.6 reduce-window.6
  24.9 0.2 slice_reduce_fusion
  25.2 0.1 mul.128
  25.5 1.4 scatter_custom_fusion
  27.0 6.7 %reduce-scatter.2.cloned.1.call-done = f32[128,2048]{1,0:T(8,128)} async-done(((f32[256,2048]{1,0:T(8,128)}), f32[128,2048]{1,0:T(8,128)}) %reduce-scatter.2.cloned.1.call-update) | async-done | bytes 1048592 | tf_op jit(solution)/shard_map/reduce_scatter | solution.py:109
  33.7 1.4 fusion.18
  35.1 1.6 fusion.22
  36.7 0.2 fusion.24
  36.9 2.5 gather_fusion
  39.4 0.2 broadcast_select_fusion
  39.6 2.6 broadcast_in_dim.36
  42.2 6.9 %all-to-all-start = ((bf16[16,64,2048]{2,1,0:T(8,128)(2,1)}), bf16[16,64,2048]{2,1,0:T(8,128)(2,1)}, u32[]{:S(2)}, u32[]{:S(2)}) async-start(bf16[16,64,2048]{2,1,0:T(8,128)(2,1)} %bitcast.60), calls=%async_computation.1 | async-start | bytes 8388608 | tf_op jit(solution)/shard_map/all_to_all | solution.py:142
  49.1 0.2 all-gather.11.cloned.1.call-start
  49.4 0.3 all-gather.11.cloned.1.call-update
  49.7 4.9 %all-gather.9.cloned.1.call-done = bf16[1,2048,1792]{2,1,0:T(8,128)(2,1)} async-done(((bf16[1,2048,896]{2,1,0:T(8,128)(2,1)}), bf16[1,2048,1792]{2,1,0:T(8,128)(2,1)}) %all-gather.9.cloned.1.call-update) | async-done | bytes 7340048 | tf_op jit(solution)/shard_map/all_gather | solution.py:137
  54.6 90.1 %all-to-all-done = bf16[16,64,2048]{2,1,0:T(8,128)(2,1)} async-done(((bf16[16,64,2048]{2,1,0:T(8,128)(2,1)}), bf16[16,64,2048]{2,1,0:T(8,128)(2,1)}, u32[]{:S(2)}, u32[]{:S(2)}) %all-to-all-start) | async-done | bytes 4194336 | tf_op jit(solution)/shard_map/all_to_all | solution.py:142
  144.7 9.8 %fusion.4 = f32[1024,896]{1,0:T(8,128)} fusion(bf16[1024,2048]{1,0:T(8,128)(2,1)} %bitcast.10, bf16[2048,1792]{1,0:T(8,128)(2,1)} %bitcast.66), kind=kOutput, calls=%fused_computation.11 | convolution fusion | flops 3758096384 | bytes 11534336 | tf_op jit(solution)/shard_map/dot_general | solution.py:46
  154.5 8.5 %fusion.9 = f32[1024,896]{1,0:T(8,128)} fusion(bf16[1024,2048]{1,0:T(8,128)(2,1)} %bitcast.10, bf16[2048,1792]{1,0:T(8,128)(2,1)S(1)} %bitcast.67), kind=kOutput, calls=%fused_computation.17 | convolution fusion | flops 3758096384 | bytes 11534336 | tf_op jit(solution)/shard_map/dot_general | solution.py:46
  163.0 9.2 %multiply_convert_fusion = bf16[1024,896]{1,0:T(8,128)(2,1)S(1)} fusion(f32[1024,896]{1,0:T(8,128)} %fusion.4, bf16[1024,2048]{1,0:T(8,128)(2,1)} %bitcast.10, bf16[2048,1792]{1,0:T(8,128)(2,1)} %bitcast.68), kind=kOutput, calls=%fused_computation.21 | convolution fusion | flops 3763601408 | bytes 13369344 | tf_op jit(solution)/shard_map/dot_general | solution.py:43
  172.2 8.7 %multiply_convert_fusion.1 = bf16[1024,896]{1,0:T(8,128)(2,1)} fusion(f32[1024,896]{1,0:T(8,128)S(1)} %copy-done.15, bf16[1024,2048]{1,0:T(8,128)(2,1)} %bitcast.10, bf16[2048,1792]{1,0:T(8,128)(2,1)S(1)} %bitcast.69), kind=kOutput, calls=%fused_computation.22 | convolution fusion | flops 3763601408 | bytes 13369344 | tf_op jit(solution)/shard_map/dot_general | solution.py:43
  180.9 7.2 %fusion.8 = bf16[1024,2048]{1,0:T(8,128)(2,1)S(1)} fusion(bf16[1024,896]{1,0:T(8,128)(2,1)} %multiply_convert_fusion.1, bf16[1,1792,2048]{2,1,0:T(8,128)(2,1)} %all-gather.11.cloned.1.call-done), kind=kOutput, calls=%fused_computation.16 | convolution fusion | flops 3758096384 | bytes 9699328 | tf_op jit(solution)/shard_map/dot_general | solution.py:50
  188.2 6.1 %add_convert_fusion = bf16[1024,2048]{1,0:T(8,128)(2,1)} fusion(bf16[1024,2048]{1,0:T(8,128)(2,1)S(1)} %fusion.8, bf16[1024,896]{1,0:T(8,128)(2,1)S(1)} %multiply_convert_fusion, bf16[1,1792,2048]{2,1,0:T(8,128)(2,1)S(1)} %copy-done.14), kind=kOutput, calls=%fused_computation.3 | convolution fusion | flops 3768582144 | bytes 13893632 | tf_op jit(solution)/shard_map/dot_general | solution.py:50
  194.3 5.3 %all-to-all-start.1 = ((bf16[16,64,2048]{2,1,0:T(8,128)(2,1)}), bf16[16,64,2048]{2,1,0:T(8,128)(2,1)}, u32[]{:S(2)}, u32[]{:S(2)}) async-start(bf16[16,64,2048]{2,1,0:T(8,128)(2,1)} %bitcast.62), calls=%async_computation.2 | async-start | bytes 8388608 | tf_op jit(solution)/shard_map/all_to_all | solution.py:148
  199.7 92.7 %all-to-all-done.1 = bf16[16,64,2048]{2,1,0:T(8,128)(2,1)} async-done(((bf16[16,64,2048]{2,1,0:T(8,128)(2,1)}), bf16[16,64,2048]{2,1,0:T(8,128)(2,1)}, u32[]{:S(2)}, u32[]{:S(2)}) %all-to-all-start.1) | async-done | bytes 4194336 | tf_op jit(solution)/shard_map/all_to_all | solution.py:148
  292.4 3.3 %convert.12 = f32[8,2,64,2048]{3,2,1,0:T(8,128)S(1)} convert(bf16[8,2,64,2048]{3,2,1,0:T(8,128)(2,1)} %bitcast.17) | non-fusion elementwise | flops 2097152 | bytes 12582912 | tf_op jit(solution)/shard_map/reshape | solution.py:149
  295.7 0.6 fusion.17
  296.3 2.3 gather_fusion.1
  298.7 2.5 reshape.142
  301.2 3.2 %multiply_reduce_fusion = f32[128,2048]{1,0:T(8,128)S(1)} fusion(f32[128,2,2048]{2,1,0:T(2,128)S(1)} %reshape.142, f32[128,2]{1,0:T(8,128)S(1)} %copy.23), kind=kLoop, calls=%fused_computation.24 | loop fusion | flops 786432 | bytes 3146752 | tf_op jit(solution)/shard_map/reduce_sum | solution.py:153
  304.3 0.2 multiply_reduce_fusion.1
  304.5 1.0 fusion.25
  (58 shorter events, 1.1 us)
Async XLA Ops:
  6.5 9.9 %copy-start = (bf16[2,512,512]{2,1,0:T(8,128)(2,1)S(1)}, bf16[2,512,512]{2,1,0:T(8,128)(2,1)}, u32[]{:S(2)}) copy-start(bf16[2,512,512]{2,1,0:T(8,128)(2,1)} %param.15) | copy-start | bytes 3145732
  6.5 27.1 %reduce-scatter.2.cloned.1.call-start = ((), (), s32[]{:S(2)}) async-start(), calls=%async_computation.3 | async-start | bytes 3145728 | tf_op jit(solution)/shard_map/reduce_scatter | solution.py:109
  7.4 5.8 %collective-permute-start = (bf16[16,1024]{1,0:T(8,128)(2,1)S(1)}, bf16[16,1024]{1,0:T(8,128)(2,1)S(1)}, u32[]{:S(2)}, u32[]{:S(2)}) collective-permute-start(bf16[16,1024]{1,0:T(8,128)(2,1)S(1)} %slice.99), channel_id=1, source_target_pairs={{0,2},{2,4},{4,6},{6,8},{8,10},{10,12},{12,14},{14,16},{16,18},{18... | collective-permute-start | bytes 98312 | tf_op jit(solution)/shard_map/ppermute | solution.py:16
  14.7 1.0 copy-start.4
  16.1 1.1 copy-start.9
  22.3 1.5 copy-start.10
  22.3 12.7 %copy-start.5 = (bf16[128,2048]{1,0:T(8,128)(2,1)S(1)}, bf16[128,2048]{1,0:T(8,128)(2,1)}, u32[]{:S(2)}) copy-start(bf16[128,2048]{1,0:T(8,128)(2,1)} %param.13) | copy-start | bytes 1572868
  22.3 12.7 %copy-start.6 = (f32[2048]{0:T(1024)S(1)}, f32[2048]{0:T(1024)}, u32[]{:S(2)}) copy-start(f32[2048]{0:T(1024)} %param.18) | copy-start | bytes 24580
  22.3 32.3 %all-gather.9.cloned.1.call-start = ((), (), s32[]{:S(2)}) async-start(), calls=%async_computation.5 | async-start | bytes 11010048 | tf_op jit(solution)/shard_map/all_gather | solution.py:137
  23.1 13.6 %copy-start.7 = (f32[2048]{0:T(1024)S(1)}, f32[2048]{0:T(1024)}, u32[]{:S(2)}) copy-start(f32[2048]{0:T(1024)} %param.19) | copy-start | bytes 24580
  23.1 139.9 %all-gather.7.cloned.1.call-start = ((), (), s32[]{:S(2)}) async-start(), calls=%async_computation.4 | async-start | bytes 11010048 | tf_op jit(solution)/shard_map/all_gather | solution.py:136
  36.7 2.7 copy-start.2
  42.2 102.5 %all-to-all-start = ((bf16[16,64,2048]{2,1,0:T(8,128)(2,1)}), bf16[16,64,2048]{2,1,0:T(8,128)(2,1)}, u32[]{:S(2)}, u32[]{:S(2)}) async-start(bf16[16,64,2048]{2,1,0:T(8,128)(2,1)} %bitcast.60), calls=%async_computation.1 | async-start | bytes 8388608 | tf_op jit(solution)/shard_map/all_to_all | solution.py:142
  49.1 131.8 %all-gather.11.cloned.1.call-start = ((), (), s32[]{:S(2)}) async-start(), calls=%async_computation.6 | async-start | bytes 11010048 | tf_op jit(solution)/shard_map/all_gather | solution.py:139
  144.7 9.8 %copy-start.12 = (bf16[1,2048,1792]{2,1,0:T(8,128)(2,1)S(1)}, bf16[1,2048,1792]{2,1,0:T(8,128)(2,1)}, u32[]{:S(2)}) copy-start(bf16[1,2048,1792]{2,1,0:T(8,128)(2,1)} %all-gather.9.cloned.1.call-done) | copy-start | bytes 22020100
  163.0 9.2 %copy-start.13 = (bf16[1,2048,1792]{2,1,0:T(8,128)(2,1)S(1)}, bf16[1,2048,1792]{2,1,0:T(8,128)(2,1)}, u32[]{:S(2)}) copy-start(bf16[1,2048,1792]{2,1,0:T(8,128)(2,1)} %all-gather.7.cloned.1.call-done) | copy-start | bytes 22020100
  163.0 9.3 %copy-start.15 = (f32[1024,896]{1,0:T(8,128)S(1)}, f32[1024,896]{1,0:T(8,128)}, u32[]{:S(2)}) copy-start(f32[1024,896]{1,0:T(8,128)} %fusion.9) | copy-start | bytes 11010052
  180.9 7.2 %copy-start.14 = (bf16[1,1792,2048]{2,1,0:T(8,128)(2,1)S(1)}, bf16[1,1792,2048]{2,1,0:T(8,128)(2,1)}, u32[]{:S(2)}) copy-start(bf16[1,1792,2048]{2,1,0:T(8,128)(2,1)} %all-gather.11.cloned.1.call-done) | copy-start | bytes 22020100
  194.3 5.3 %copy-start.11 = (f32[128,2]{0,1:T(2,128)S(1)}, f32[128,2]{0,1:T(2,128)}, u32[]{:S(2)}) copy-start(f32[128,2]{0,1:T(2,128)} %param.22) | copy-start | bytes 3076
  194.3 98.1 %all-to-all-start.1 = ((bf16[16,64,2048]{2,1,0:T(8,128)(2,1)}), bf16[16,64,2048]{2,1,0:T(8,128)(2,1)}, u32[]{:S(2)}, u32[]{:S(2)}) async-start(bf16[16,64,2048]{2,1,0:T(8,128)(2,1)} %bitcast.62), calls=%async_computation.2 | async-start | bytes 8388608 | tf_op jit(solution)/shard_map/all_to_all | solution.py:148
  298.7 5.8 %copy-start.8 = (f32[2048]{0:T(1024)S(1)}, f32[2048]{0:T(1024)}, u32[]{:S(2)}) copy-start(f32[2048]{0:T(1024)} %param.20) | copy-start | bytes 24580
  298.7 6.9 %copy-start.1 = (bf16[2,512,512]{2,1,0:T(8,128)(2,1)S(1)}, bf16[2,512,512]{2,1,0:T(8,128)(2,1)}, u32[]{:S(2)}) copy-start(bf16[2,512,512]{2,1,0:T(8,128)(2,1)} %param.15) | copy-start | bytes 3145732
  301.1 3.4 %copy-start.3 = (bf16[128,2048]{1,0:T(8,128)(2,1)S(1)}, bf16[128,2048]{1,0:T(8,128)(2,1)}, u32[]{:S(2)}) copy-start(bf16[128,2048]{1,0:T(8,128)(2,1)} %copy-done.2) | copy-start | bytes 1572868
Sparse Core Ops, SparseCore 0:
  22.4 11.2 reduce-scatter.1
  35.2 19.3 all-gather.8
  56.2 19.3 all-gather.6
  77.0 19.4 all-gather.10
where the time goes:
time: 313 us; the launch traced here: 312 us
  waiting for transfers between devices  198 us (63%)
  matrix products  54.8 us (18%)
  starting transfers between devices  15.9 us (5%)
  other arithmetic  15 us (5%)
  local copies, waits for them, and re-layouts  14.3 us (5%)
  between operations  13.6 us (4%)
    all_to_all x1, waiting for transfers between devices, body(): lax.all_to_all(summed_half, 'sp', split_axis=0, concat_axis=0, tiled=True)  92.7 us
    all_to_all x1, waiting for transfers between devices, body(): lax.all_to_all(send_rows, 'sp', split_axis=0, concat_axis=0, tiled=True)  90.1 us
    dot_general x2, matrix products, expert_whole_half(): jnp.dot(flat_rows, up_full[:, low:low + quarter], preferred_element_type=...  18.2 us
    dot_general x2, matrix products, expert_whole_half(): jnp.dot(flat_rows, gate_full[:, low:low + quarter], preferred_element_typ...  17.9 us
    dot_general x2, matrix products, expert_whole_half(): jnp.dot(active, down_full[low:low + quarter], preferred_element_type=jnp....  13.3 us
    all_to_all x1, starting transfers between devices, body(): lax.all_to_all(send_rows, 'sp', split_axis=0, concat_axis=0, tiled=True)  6.94 us
    reduce_scatter x1, waiting for transfers between devices, body(): lax.psum_scatter(jnp.dot(scaled, weight_rows, preferred_element_type=jnp....  6.67 us
  transfers between devices with their start and end apart: 7, of which 5 were waited for; matrix products, arithmetic and copies ran while one was open for 15% of the time, Pallas kernels for 0%

commit v1 on v0

--- a/solution.py
+++ b/solution.py
@@ -5,6 +5,7 @@
 
 GROUPS = 4
 TOP = 2
+CHUNKS = 2
 
 
 EPS = 1e-06
@@ -34,24 +35,13 @@
     return levels
 
 
-def expert_whole_half(token_rows, gate_full, up_full, down_full, parts):
+def expert_half(token_rows, gate_full, up_full, down_full):
     flat_rows = token_rows.reshape(-1, token_rows.shape[-1])
-    quarter = gate_full.shape[1] // parts
-    total = jnp.zeros(flat_rows.shape, jnp.float32)
-    for part_id in range(parts):
-        low = part_id * quarter
-        gate_value = jnp.dot(
-            flat_rows, gate_full[:, low : low + quarter], preferred_element_type=jnp.float32
-        )
-        up_value = jnp.dot(
-            flat_rows, up_full[:, low : low + quarter], preferred_element_type=jnp.float32
-        )
-        active = (jax.nn.silu(gate_value) * up_value).astype(jnp.bfloat16)
-        term = jnp.dot(
-            active, down_full[low : low + quarter], preferred_element_type=jnp.float32
-        ).astype(jnp.bfloat16)
-        total = total + term.astype(jnp.float32)
-    return total.astype(jnp.bfloat16).reshape(token_rows.shape)
+    gate_value = jnp.dot(flat_rows, gate_full, preferred_element_type=jnp.float32)
+    up_value = jnp.dot(flat_rows, up_full, preferred_element_type=jnp.float32)
+    active = (jax.nn.silu(gate_value) * up_value).astype(jnp.bfloat16)
+    half = jnp.dot(active, down_full, preferred_element_type=jnp.float32)
+    return half.astype(jnp.bfloat16).reshape(token_rows.shape)
 
 
 def body(
@@ -137,17 +127,32 @@
         lax.all_gather(up_part, "tp", axis=1, tiled=True),
     )
     down_full = lax.all_gather(down_part, "tp", axis=0, tiled=True)
-    send_rows = jnp.repeat(table.reshape(experts_all, capacity, model_width), 2, axis=0)
-    summed_half = expert_whole_half(
-        lax.all_to_all(send_rows, "sp", split_axis=0, concat_axis=0, tiled=True),
-        gate_full,
-        up_full,
-        down_full,
-        tp_count,
-    )
-    returned = lax.all_to_all(summed_half, "sp", split_axis=0, concat_axis=0, tiled=True)
-    pairs = returned.astype(jnp.float32).reshape(experts_all, 2, capacity, model_width)
-    results = lax.optimization_barrier((pairs[:, 0] + pairs[:, 1]).astype(jnp.bfloat16))
+    sp_count = lax.axis_size("sp")
+    same_half = [[2 * e + h for e in range(experts_all)] for h in range(2)]
+    swap = [(i, i ^ 1) for i in range(sp_count)]
+
+    def exchange(rows):
+        return lax.all_to_all(
+            rows,
+            "sp",
+            split_axis=0,
+            concat_axis=0,
+            axis_index_groups=same_half,
+            tiled=True,
+        )
+
+    table = table.reshape(experts_all, capacity, model_width)
+    step = capacity // CHUNKS
+    returned = []
+    for chunk in range(CHUNKS):
+        own = exchange(table[:, chunk * step : (chunk + 1) * step])
+        other = lax.ppermute(own, "sp", swap)
+        own_half = expert_half(own, gate_full, up_full, down_full)
+        other_half = expert_half(other, gate_full, up_full, down_full)
+        peer_half = lax.ppermute(other_half, "sp", swap)
+        summed = own_half.astype(jnp.float32) + peer_half.astype(jnp.float32)
+        returned.append(exchange(summed.astype(jnp.bfloat16)))
+    results = jnp.concatenate(returned, 1)
     picked = results.reshape(experts_all * capacity, model_width)[target].astype(jnp.float32)
     weighted = picked * route_weight.reshape(-1)[:, None]
     ffn_sum = jnp.sum(weighted.reshape(row_count, TOP, model_width), 1)

time: 313 us -> 241 us (0.77)
  the two profiles are of different devices: /device:TPU:14 before, /device:TPU:0 now
where the time goes in v1:
time: 241 us; the launch traced here: 240 us
  matrix products  75.5 us (31%)
  waiting for transfers between devices  70.7 us (29%)
  blocking collectives  31.7 us (13%)
  starting transfers between devices  21.9 us (9%)
  other arithmetic  15.2 us (6%)
  between operations  13.6 us (6%)
  local copies, waits for them, and re-layouts  11.8 us (5%)
    all_to_all x3, waiting for transfers between devices, exchange(): lax.all_to_all(rows, 'sp', split_axis=0, concat_axis=0, axis_index_groups...  54.2 us
    dot_general x4, matrix products, expert_half(): half = jnp.dot(active, down_full, preferred_element_type=jnp.float32)  44 us
    all_to_all x1, blocking collectives, exchange(): lax.all_to_all(rows, 'sp', split_axis=0, concat_axis=0, axis_index_groups...  31.7 us
    dot_general x2, matrix products, expert_half(): up_value = jnp.dot(flat_rows, up_full, preferred_element_type=jnp.float32)  13.2 us
    dot_general x2, matrix products, expert_half(): jnp.dot(flat_rows, gate_full, preferred_element_type=jnp.float32)  13.1 us
    all_to_all x3, starting transfers between devices, exchange(): lax.all_to_all(rows, 'sp', split_axis=0, concat_axis=0, axis_index_groups...  11.9 us
    reduce_scatter x1, waiting for transfers between devices, body(): lax.psum_scatter(jnp.dot(scaled, weight_rows, preferred_element_type=jnp....  6.67 us
    ppermute x2, waiting for transfers between devices, body(): other = lax.ppermute(own, 'sp', swap)  6.4 us
  transfers between devices with their start and end apart: 12, of which 6 were waited for; matrix products, arithmetic and copies ran while one was open for 35% of the time, Pallas kernels for 0%

profile of v1, /device:TPU:0, one launch (start us, length us, event | category | flops | bytes accessed | tf_op | source)
XLA Modules:
  0.0 240.4 jit_solution(13857787919653534314)
XLA Ops:
  6.5 0.8 slice.81
  7.4 4.9 %collective-permute-start = (bf16[16,1024]{1,0:T(8,128)(2,1)S(1)}, bf16[16,1024]{1,0:T(8,128)(2,1)S(1)}, u32[]{:S(2)}, u32[]{:S(2)}) collective-permute-start(bf16[16,1024]{1,0:T(8,128)(2,1)S(1)} %slice.81), channel_id=1, source_target_pairs={{0,2},{2,4},{4,6},{6,8},{8,10},{10,12},{12,14},{14,16},{16,18},{18... | collective-permute-start | bytes 98312 | tf_op jit(solution)/shard_map/ppermute | solution.py:17
  12.3 1.5 collective-permute-done
  13.8 1.2 maximum_convert_fusion
  15.7 0.9 copy-done.4
  16.6 0.3 fusion.92
  16.9 0.3 fusion.93
  17.3 0.4 convolution_bitcast_fusion
  17.7 0.3 copy.15
  18.3 4.8 %fusion.24 = f32[256,2048]{1,0:T(8,128)} fusion(bf16[256,1024]{0,1:T(8,128)(2,1)S(1)} %fusion.60, bf16[2048,2048]{1,0:T(8,128)(2,1)} %param.17, s32[]{:T(128)S(6)} %select_n.124), kind=kOutput, calls=%fused_computation.27 | convolution fusion | flops 1073741824 | bytes 6815748 | tf_op jit(solution)/shard_map/dot_general | solution.py:100
  23.2 0.7 all-gather.9.cloned.1.call-update
  23.9 0.7 all-gather.11.cloned.1.call-update
  24.7 0.5 all-gather.7.cloned.1.call-update
  25.7 0.6 reduce-window.6
  26.9 1.4 scatter_custom_fusion
  28.4 6.7 %reduce-scatter.2.cloned.1.call-done = f32[128,2048]{1,0:T(8,128)} async-done(((f32[256,2048]{1,0:T(8,128)}), f32[128,2048]{1,0:T(8,128)}) %reduce-scatter.2.cloned.1.call-update) | async-done | bytes 1048592 | tf_op jit(solution)/shard_map/reduce_scatter | solution.py:99
  35.1 1.4 fusion.52
  36.5 1.6 fusion.56
  38.1 0.8 copy-done.2
  39.1 2.5 %gather_fusion = bf16[512,2048]{1,0:T(8,128)(2,1)S(1)} fusion(bf16[128,2048]{1,0:T(8,128)(2,1)S(1)} %fusion.58, s32[1024]{0:T(1024)S(1)} %pad_clamp_fusion.1), kind=kCustom, calls=%fused_computation | custom fusion | bytes 4196352 | tf_op jit(solution)/shard_map/gather | solution.py:120
  41.8 1.1 fusion.107
  42.9 31.7 %all_to_all.20 = bf16[8,32,2048]{2,1,0:T(8,128)(2,1)S(1)} all-to-all(bf16[8,32,2048]{2,1,0:T(8,128)(2,1)S(1)} %get-tuple-element.7), channel_id=1, replica_groups={{0,4,8,12,16,20,24,28},{2,6,10,14,18,22,26,30},{1,5,9,13,17,21,25,29},{..., dimensions={0} | all-to-all | bytes 2097152 | tf_op jit(solution)/shard_map/all_to_all | solution.py:135
  74.6 3.7 %all-to-all-start.2 = ((bf16[8,32,2048]{2,1,0:T(8,128)(2,1)}), bf16[8,32,2048]{2,1,0:T(8,128)(2,1)S(1)}, u32[]{:S(2)}, u32[]{:S(2)}) async-start(bf16[8,32,2048]{2,1,0:T(8,128)(2,1)} %get-tuple-element.8), calls=%async_computation.3 | async-start | bytes 2097152 | tf_op jit(solution)/shard_map/all_to_all | solution.py:135
  78.4 1.5 collective-permute-start.1
  79.9 23.9 %all-to-all-done.2 = bf16[8,32,2048]{2,1,0:T(8,128)(2,1)S(1)} async-done(((bf16[8,32,2048]{2,1,0:T(8,128)(2,1)}), bf16[8,32,2048]{2,1,0:T(8,128)(2,1)S(1)}, u32[]{:S(2)}, u32[]{:S(2)}) %all-to-all-start.2) | async-done | bytes 1048608 | tf_op jit(solution)/shard_map/all_to_all | solution.py:135
  103.8 1.5 collective-permute-start.3
  105.3 6.4 %fusion.12 = f32[256,1792]{1,0:T(8,128)} fusion(bf16[256,2048]{1,0:T(8,128)(2,1)S(1)} %bitcast.109, bf16[1,2048,1792]{2,1,0:T(8,128)(2,1)} %all-gather.9.cloned.1.call-done), kind=kOutput, calls=%fused_computation.15 | convolution fusion | flops 1879048192 | bytes 10223616 | tf_op jit(solution)/shard_map/dot_general | solution.py:41
  111.7 11.3 %fusion.35 = bf16[256,2048]{1,0:T(8,128)(2,1)} fusion(bf16[1,1792,2048]{2,1,0:T(8,128)(2,1)} %all-gather.11.cloned.1.call-done, f32[256,1792]{1,0:T(8,128)} %fusion.12, bf16[256,2048]{1,0:T(8,128)(2,1)S(1)} %bitcast.110, bf16[1,2048,1792]{2,1,0:T(8,128)(2,1)} %all-gather.7.cloned.1.call-done), kind=kOutput, calls=%fused_computation.32 | convolution fusion | flops 3761373184 | bytes 18612224 | tf_op jit(solution)/shard_map/dot_general | solution.py:43
  123.0 0.6 collective-permute-start.2
  123.6 6.4 %collective-permute-done.3 = bf16[8,32,2048]{2,1,0:T(8,128)(2,1)} collective-permute-done((bf16[8,32,2048]{2,1,0:T(8,128)(2,1)S(1)}, bf16[8,32,2048]{2,1,0:T(8,128)(2,1)}, u32[]{:S(2)}, u32[]{:S(2)}) %collective-permute-start.3) | collective-permute-done | bytes 1048608 | tf_op jit(solution)/shard_map/ppermute | solution.py:149
  130.0 6.8 %fusion.8 = f32[256,1792]{1,0:T(8,128)} fusion(bf16[256,2048]{1,0:T(8,128)(2,1)} %bitcast.18, bf16[1,2048,1792]{2,1,0:T(8,128)(2,1)} %all-gather.9.cloned.1.call-done), kind=kOutput, calls=%fused_computation.11 | convolution fusion | flops 1879048192 | bytes 10223616 | tf_op jit(solution)/shard_map/dot_general | solution.py:41
  136.7 11.6 %fusion.41 = bf16[256,2048]{1,0:T(8,128)(2,1)} fusion(bf16[1,1792,2048]{2,1,0:T(8,128)(2,1)} %all-gather.11.cloned.1.call-done, f32[256,1792]{1,0:T(8,128)} %fusion.8, bf16[256,2048]{1,0:T(8,128)(2,1)} %bitcast.18, bf16[1,2048,1792]{2,1,0:T(8,128)(2,1)} %all-gather.7.cloned.1.call-done), kind=kOutput, calls=%fused_computation.34 | convolution fusion | flops 3761373184 | bytes 18612224 | tf_op jit(solution)/shard_map/dot_general | solution.py:43
  148.4 1.5 collective-permute-start.4
  149.8 6.7 %fusion.22 = f32[256,1792]{1,0:T(8,128)} fusion(bf16[256,2048]{1,0:T(8,128)(2,1)S(1)} %bitcast.103, bf16[1,2048,1792]{2,1,0:T(8,128)(2,1)} %all-gather.7.cloned.1.call-done), kind=kOutput, calls=%fused_computation.25 | convolution fusion | flops 1879048192 | bytes 10223616 | tf_op jit(solution)/shard_map/dot_general | solution.py:40
  156.5 10.5 %fusion.32 = bf16[256,2048]{1,0:T(8,128)(2,1)S(1)} fusion(bf16[1,1792,2048]{2,1,0:T(8,128)(2,1)} %all-gather.11.cloned.1.call-done, bf16[256,2048]{1,0:T(8,128)(2,1)} %bitcast.104, bf16[1,2048,1792]{2,1,0:T(8,128)(2,1)} %all-gather.9.cloned.1.call-done, f32[256,1792]{1,0:T(8,128)} %fusion.22), kind=kOutput, calls=%fused_computation.31 | convolution fusion | flops 3761373184 | bytes 18612224 | tf_op jit(solution)/shard_map/dot_general | solution.py:43
  167.0 1.3 fusion.51
  168.4 3.7 %all-to-all-start.1 = ((bf16[8,32,2048]{2,1,0:T(8,128)(2,1)}), bf16[8,32,2048]{2,1,0:T(8,128)(2,1)S(1)}, u32[]{:S(2)}, u32[]{:S(2)}) async-start(bf16[8,32,2048]{2,1,0:T(8,128)(2,1)} %fusion.51), calls=%async_computation.2 | async-start | bytes 2097152 | tf_op jit(solution)/shard_map/all_to_all | solution.py:135
  172.1 6.4 %fusion.18 = f32[256,1792]{1,0:T(8,128)} fusion(bf16[256,2048]{1,0:T(8,128)(2,1)S(1)} %bitcast.102, bf16[1,2048,1792]{2,1,0:T(8,128)(2,1)} %all-gather.7.cloned.1.call-done), kind=kOutput, calls=%fused_computation.21 | convolution fusion | flops 1879048192 | bytes 10223616 | tf_op jit(solution)/shard_map/dot_general | solution.py:40
  178.5 10.5 %fusion.38 = bf16[256,2048]{1,0:T(8,128)(2,1)S(1)} fusion(bf16[1,1792,2048]{2,1,0:T(8,128)(2,1)} %all-gather.11.cloned.1.call-done, bf16[256,2048]{1,0:T(8,128)(2,1)} %bitcast.101, bf16[1,2048,1792]{2,1,0:T(8,128)(2,1)} %all-gather.9.cloned.1.call-done, f32[256,1792]{1,0:T(8,128)} %fusion.18), kind=kOutput, calls=%fused_computation.33 | convolution fusion | flops 3761373184 | bytes 18612224 | tf_op jit(solution)/shard_map/dot_general | solution.py:43
  189.1 1.4 fusion.50
  190.5 5.6 %all-to-all-done.1 = bf16[8,32,2048]{2,1,0:T(8,128)(2,1)S(1)} async-done(((bf16[8,32,2048]{2,1,0:T(8,128)(2,1)}), bf16[8,32,2048]{2,1,0:T(8,128)(2,1)S(1)}, u32[]{:S(2)}, u32[]{:S(2)}) %all-to-all-start.1) | async-done | bytes 1048608 | tf_op jit(solution)/shard_map/all_to_all | solution.py:135
  196.1 4.5 %all-to-all-start.3 = ((bf16[8,32,2048]{2,1,0:T(8,128)(2,1)}), bf16[8,32,2048]{2,1,0:T(8,128)(2,1)}, u32[]{:S(2)}, u32[]{:S(2)}) async-start(bf16[8,32,2048]{2,1,0:T(8,128)(2,1)} %fusion.50), calls=%async_computation.4 | async-start | bytes 2097152 | tf_op jit(solution)/shard_map/all_to_all | solution.py:135
  200.7 24.7 %all-to-all-done.3 = bf16[8,32,2048]{2,1,0:T(8,128)(2,1)} async-done(((bf16[8,32,2048]{2,1,0:T(8,128)(2,1)}), bf16[8,32,2048]{2,1,0:T(8,128)(2,1)}, u32[]{:S(2)}, u32[]{:S(2)}) %all-to-all-start.3) | async-done | bytes 1048608 | tf_op jit(solution)/shard_map/all_to_all | solution.py:135
  225.4 1.4 pad_maximum_fusion
  226.7 1.4 gather_fusion.1
  228.1 1.3 reshape.150
  229.5 3.2 %multiply_reduce_fusion = f32[128,2048]{1,0:T(8,128)S(1)} fusion(f32[128,2,2048]{2,1,0:T(2,128)S(1)} %reshape.150, f32[128,2]{1,0:T(8,128)S(1)} %copy.19), kind=kLoop, calls=%fused_computation.42 | loop fusion | flops 786432 | bytes 3146752 | tf_op jit(solution)/shard_map/reduce_sum | solution.py:158
  232.8 1.0 fusion.59
  (70 shorter events, 3.0 us)
Async XLA Ops:
  6.5 10.7 %copy-start = (bf16[2,512,512]{2,1,0:T(8,128)(2,1)S(1)}, bf16[2,512,512]{2,1,0:T(8,128)(2,1)}, u32[]{:S(2)}) copy-start(bf16[2,512,512]{2,1,0:T(8,128)(2,1)} %param.15) | copy-start | bytes 3145732
  6.5 28.6 %reduce-scatter.2.cloned.1.call-start = ((), (), s32[]{:S(2)}) async-start(), calls=%async_computation.5 | async-start | bytes 3145728 | tf_op jit(solution)/shard_map/reduce_scatter | solution.py:99
  7.4 6.4 %collective-permute-start = (bf16[16,1024]{1,0:T(8,128)(2,1)S(1)}, bf16[16,1024]{1,0:T(8,128)(2,1)S(1)}, u32[]{:S(2)}, u32[]{:S(2)}) collective-permute-start(bf16[16,1024]{1,0:T(8,128)(2,1)S(1)} %slice.81), channel_id=1, source_target_pairs={{0,2},{2,4},{4,6},{6,8},{8,10},{10,12},{12,14},{14,16},{16,18},{18... | collective-permute-start | bytes 98312 | tf_op jit(solution)/shard_map/ppermute | solution.py:17
  15.6 1.0 copy-start.4
  17.2 0.8 copy-start.12
  23.1 82.2 %all-gather.9.cloned.1.call-start = ((), (), s32[]{:S(2)}) async-start(), calls=%async_computation.7 | async-start | bytes 11010048 | tf_op jit(solution)/shard_map/all_gather | solution.py:127
  23.9 87.9 %all-gather.11.cloned.1.call-start = ((), (), s32[]{:S(2)}) async-start(), calls=%async_computation.8 | async-start | bytes 11010048 | tf_op jit(solution)/shard_map/all_gather | solution.py:129
  24.6 0.7 copy-start.13
  24.6 11.9 %copy-start.8 = (bf16[128,2048]{1,0:T(8,128)(2,1)S(1)}, bf16[128,2048]{1,0:T(8,128)(2,1)}, u32[]{:S(2)}) copy-start(bf16[128,2048]{1,0:T(8,128)(2,1)} %param.13) | copy-start | bytes 1572868
  24.6 11.9 %copy-start.9 = (f32[2048]{0:T(1024)S(1)}, f32[2048]{0:T(1024)}, u32[]{:S(2)}) copy-start(f32[2048]{0:T(1024)} %param.18) | copy-start | bytes 24580
  24.6 87.1 %all-gather.7.cloned.1.call-start = ((), (), s32[]{:S(2)}) async-start(), calls=%async_computation.6 | async-start | bytes 11010048 | tf_op jit(solution)/shard_map/all_gather | solution.py:126
  25.3 13.6 %copy-start.10 = (f32[2048]{0:T(1024)S(1)}, f32[2048]{0:T(1024)}, u32[]{:S(2)}) copy-start(f32[2048]{0:T(1024)} %param.19) | copy-start | bytes 24580
  38.1 0.8 copy-start.2
  74.6 75.2 %copy-start.7 = (bf16[8,32,2048]{2,1,0:T(8,128)(2,1)}, bf16[8,32,2048]{2,1,0:T(8,128)(2,1)S(1)}, u32[]{:S(2)}) copy-start(bf16[8,32,2048]{2,1,0:T(8,128)(2,1)S(1)} %all_to_all.20) | copy-start | bytes 3145732
  74.6 29.2 %all-to-all-start.2 = ((bf16[8,32,2048]{2,1,0:T(8,128)(2,1)}), bf16[8,32,2048]{2,1,0:T(8,128)(2,1)S(1)}, u32[]{:S(2)}, u32[]{:S(2)}) async-start(bf16[8,32,2048]{2,1,0:T(8,128)(2,1)} %get-tuple-element.8), calls=%async_computation.3 | async-start | bytes 2097152 | tf_op jit(solution)/shard_map/all_to_all | solution.py:135
  78.4 26.9 %collective-permute-start.1 = (bf16[8,32,2048]{2,1,0:T(8,128)(2,1)S(1)}, bf16[8,32,2048]{2,1,0:T(8,128)(2,1)S(1)}, u32[]{:S(2)}, u32[]{:S(2)}) collective-permute-start(bf16[8,32,2048]{2,1,0:T(8,128)(2,1)S(1)} %all_to_all.20), channel_id=1, source_target_pairs={{0,2},{2,0},{4,6},{6,4},{8,10},{10,8},{12,14},{14,12},{16,18},{18,... | collective-permute-start | bytes 3145736 | tf_op jit(solution)/shard_map/ppermute | solution.py:149
  103.8 7.9 %copy-start.5 = (bf16[8,32,2048]{2,1,0:T(8,128)(2,1)}, bf16[8,32,2048]{2,1,0:T(8,128)(2,1)S(1)}, u32[]{:S(2)}) copy-start(bf16[8,32,2048]{2,1,0:T(8,128)(2,1)S(1)} %all-to-all-done.2) | copy-start | bytes 3145732
  103.8 26.1 %collective-permute-start.3 = (bf16[8,32,2048]{2,1,0:T(8,128)(2,1)S(1)}, bf16[8,32,2048]{2,1,0:T(8,128)(2,1)}, u32[]{:S(2)}, u32[]{:S(2)}) collective-permute-start(bf16[8,32,2048]{2,1,0:T(8,128)(2,1)S(1)} %all-to-all-done.2), channel_id=1, source_target_pairs={{0,2},{2,0},{4,6},{6,4},{8,10},{10,8},{12,14},{14,12},{16,18},{18,... | collective-permute-start | bytes 3145736 | tf_op jit(solution)/shard_map/ppermute | solution.py:149
  123.0 44.0 %collective-permute-start.2 = (bf16[8,32,2048]{2,1,0:T(8,128)(2,1)}, bf16[8,32,2048]{2,1,0:T(8,128)(2,1)S(1)}, u32[]{:S(2)}, u32[]{:S(2)}) collective-permute-start(bf16[8,32,2048]{2,1,0:T(8,128)(2,1)} %bitcast.111), channel_id=1, source_target_pairs={{0,2},{2,0},{4,6},{6,4},{8,10},{10,8},{12,14},{14,12},{16,18},{18,... | collective-permute-start | bytes 3145736 | tf_op jit(solution)/shard_map/ppermute | solution.py:152
  148.4 40.7 %collective-permute-start.4 = (bf16[8,32,2048]{2,1,0:T(8,128)(2,1)}, bf16[8,32,2048]{2,1,0:T(8,128)(2,1)S(1)}, u32[]{:S(2)}, u32[]{:S(2)}) collective-permute-start(bf16[8,32,2048]{2,1,0:T(8,128)(2,1)} %bitcast.108), channel_id=1, source_target_pairs={{0,2},{2,0},{4,6},{6,4},{8,10},{10,8},{12,14},{14,12},{16,18},{18,... | collective-permute-start | bytes 3145736 | tf_op jit(solution)/shard_map/ppermute | solution.py:152
  168.4 3.7 %copy-start.6 = (bf16[8,32,2048]{2,1,0:T(8,128)(2,1)S(1)}, bf16[8,32,2048]{2,1,0:T(8,128)(2,1)}, u32[]{:S(2)}) copy-start(bf16[8,32,2048]{2,1,0:T(8,128)(2,1)} %copy-done.5) | copy-start | bytes 3145732
  168.4 27.7 %all-to-all-start.1 = ((bf16[8,32,2048]{2,1,0:T(8,128)(2,1)}), bf16[8,32,2048]{2,1,0:T(8,128)(2,1)S(1)}, u32[]{:S(2)}, u32[]{:S(2)}) async-start(bf16[8,32,2048]{2,1,0:T(8,128)(2,1)} %fusion.51), calls=%async_computation.2 | async-start | bytes 2097152 | tf_op jit(solution)/shard_map/all_to_all | solution.py:135
  189.1 11.5 %copy-start.14 = (f32[128,2]{0,1:T(2,128)S(1)}, f32[128,2]{0,1:T(2,128)}, u32[]{:S(2)}) copy-start(f32[128,2]{0,1:T(2,128)} %param.22) | copy-start | bytes 3076
  196.1 29.3 %all-to-all-start.3 = ((bf16[8,32,2048]{2,1,0:T(8,128)(2,1)}), bf16[8,32,2048]{2,1,0:T(8,128)(2,1)}, u32[]{:S(2)}, u32[]{:S(2)}) async-start(bf16[8,32,2048]{2,1,0:T(8,128)(2,1)} %fusion.50), calls=%async_computation.4 | async-start | bytes 2097152 | tf_op jit(solution)/shard_map/all_to_all | solution.py:135
  229.4 3.4 %copy-start.3 = (bf16[128,2048]{1,0:T(8,128)(2,1)S(1)}, bf16[128,2048]{1,0:T(8,128)(2,1)}, u32[]{:S(2)}) copy-start(bf16[128,2048]{1,0:T(8,128)(2,1)} %copy-done.2) | copy-start | bytes 1572868
  229.4 3.4 %copy-start.11 = (f32[2048]{0:T(1024)S(1)}, f32[2048]{0:T(1024)}, u32[]{:S(2)}) copy-start(f32[2048]{0:T(1024)} %param.20) | copy-start | bytes 24580
  229.5 4.4 %copy-start.1 = (bf16[2,512,512]{2,1,0:T(8,128)(2,1)S(1)}, bf16[2,512,512]{2,1,0:T(8,128)(2,1)}, u32[]{:S(2)}) copy-start(bf16[2,512,512]{2,1,0:T(8,128)(2,1)} %param.15) | copy-start | bytes 3145732
Sparse Core Ops, SparseCore 0:
  23.2 11.8 reduce-scatter.1
  36.7 19.4 all-gather.8
  57.7 19.4 all-gather.10
  78.6 19.3 all-gather.6

commit v2 on v1

--- a/solution.py
+++ b/solution.py
@@ -5,7 +5,8 @@
 
 GROUPS = 4
 TOP = 2
-CHUNKS = 2
+EDGES = (0, 2, 4)
+PARTS = 4
 
 
 EPS = 1e-06
@@ -96,12 +97,19 @@
     )
     scaled = (grouped.reshape(tokens_here, width_here) * channel_scale).astype(jnp.bfloat16)
     weight_rows = lax.dynamic_slice_in_dim(out_weight, tp_index * width_here, width_here, 0)
-    projection = lax.psum_scatter(
-        jnp.dot(scaled, weight_rows, preferred_element_type=jnp.float32),
-        "tp",
-        scatter_dimension=0,
-        tiled=True,
-    )
+    rows_here = tokens_here // tp_count
+
+    def project(owner):
+        block = lax.dynamic_slice_in_dim(scaled, owner * rows_here, rows_here, 0)
+        return jnp.dot(block, weight_rows, preferred_element_type=jnp.float32)
+
+    projection = None
+    for distance in range(1, tp_count):
+        owner = lax.rem(tp_index + distance, tp_count)
+        route = [(i, (i + distance) % tp_count) for i in range(tp_count)]
+        arrived = lax.ppermute(project(owner), "tp", route)
+        projection = arrived if projection is None else projection + arrived
+    projection = project(tp_index) + projection
     mixed = projection.astype(jnp.bfloat16)
     middle = (residual.astype(jnp.float32) + rms_scale(mixed, post_mix_gain)).astype(jnp.bfloat16)
     normed = rms_scale(middle, pre_ffn_gain).astype(jnp.bfloat16)
@@ -142,10 +150,10 @@
         )
 
     table = table.reshape(experts_all, capacity, model_width)
-    step = capacity // CHUNKS
+    bounds = [capacity * part // PARTS for part in EDGES]
     returned = []
-    for chunk in range(CHUNKS):
-        own = exchange(table[:, chunk * step : (chunk + 1) * step])
+    owns = [exchange(table[:, low:high]) for low, high in zip(bounds[:-1], bounds[1:])]
+    for own in owns:
         other = lax.ppermute(own, "sp", swap)
         own_half = expert_half(own, gate_full, up_full, down_full)
         other_half = expert_half(other, gate_full, up_full, down_full)

time: 241 us -> 232 us (0.963)
  waiting for transfers between devices: 70.7 us -> 64.5 us
  other arithmetic: 15.2 us -> 11.6 us
  matrix products: 75.5 us -> 78.4 us
    reduce_scatter x1 -> x0, waiting for transfers between devices: 6.67 us -> none  [body(): lax.psum_scatter(jnp.dot(scaled, weight_rows, preferred_element_type=jnp....]
    dot_general x1 -> x2, matrix products: 4.84 us -> 7.64 us  [project(): return jnp.dot(block, weight_rows, preferred_element_type=jnp.float32)]
    reduce_sum x3 -> x2, other arithmetic: 3.13 us -> 0.53 us  [rms_scale(): inverse = lax.rsqrt(jnp.mean(values * values, axis=-1, keepdims=True) + EPS)]
  transfers between devices with their start and end apart: 12 -> 12, of which waited for: 6 -> 6; matrix products, arithmetic and copies ran while one was open for 35% -> 39% of each run, Pallas kernels for 0% -> 0%
where the time goes in v2:
time: 232 us; the launch traced here: 231 us
  matrix products  78.4 us (34%)
  waiting for transfers between devices  64.5 us (28%)
  blocking collectives  33.1 us (14%)
  starting transfers between devices  20.4 us (9%)
  between operations  13.6 us (6%)
  other arithmetic  11.6 us (5%)
  local copies, waits for them, and re-layouts  9.68 us (4%)
    all_to_all x3, waiting for transfers between devices, exchange(): lax.all_to_all(rows, 'sp', split_axis=0, concat_axis=0, axis_index_groups...  55.3 us
    dot_general x4, matrix products, expert_half(): half = jnp.dot(active, down_full, preferred_element_type=jnp.float32)  44 us
    all_to_all x1, blocking collectives, exchange(): lax.all_to_all(rows, 'sp', split_axis=0, concat_axis=0, axis_index_groups...  33.1 us
    dot_general x2, matrix products, expert_half(): up_value = jnp.dot(flat_rows, up_full, preferred_element_type=jnp.float32)  13.2 us
    dot_general x2, matrix products, expert_half(): jnp.dot(flat_rows, gate_full, preferred_element_type=jnp.float32)  13.1 us
    all_to_all x3, starting transfers between devices, exchange(): lax.all_to_all(rows, 'sp', split_axis=0, concat_axis=0, axis_index_groups...  12 us
    dot_general x2, matrix products, project(): return jnp.dot(block, weight_rows, preferred_element_type=jnp.float32)  7.64 us
    ppermute x2, waiting for transfers between devices, body(): other = lax.ppermute(own, 'sp', swap)  6.38 us
  transfers between devices with their start and end apart: 12, of which 6 were waited for; matrix products, arithmetic and copies ran while one was open for 39% of the time, Pallas kernels for 0%

profile of v2, /device:TPU:0, one launch (start us, length us, event | category | flops | bytes accessed | tf_op | source)
XLA Modules:
  0.0 231.3 jit_solution(8156272994700348711)
XLA Ops:
  6.5 0.7 all-gather.9.cloned.1.call-update
  7.3 0.7 all-gather.11.cloned.1.call-update
  8.1 0.2 copy-done.4
  8.3 4.9 %collective-permute-start = (bf16[16,1024]{1,0:T(8,128)(2,1)S(1)}, bf16[16,1024]{1,0:T(8,128)(2,1)S(1)}, u32[]{:S(2)}, u32[]{:S(2)}) collective-permute-start(bf16[16,1024]{1,0:T(8,128)(2,1)S(1)} %slice.81), channel_id=1, source_target_pairs={{0,2},{2,4},{4,6},{6,8},{8,10},{10,12},{12,14},{14,16},{16,18},{18... | collective-permute-start | bytes 98312 | tf_op jit(solution)/shard_map/ppermute | solution.py:18
  13.6 0.6 reduce-window.6
  14.2 0.6 collective-permute-done
  15.6 0.3 fusion.101
  15.9 0.3 fusion.102
  16.2 0.4 convolution_bitcast_fusion
  16.7 0.3 copy.15
  17.0 0.2 fusion.67
  17.2 3.6 %fusion.24 = f32[128,2048]{1,0:T(8,128)S(1)} fusion(bf16[2048,2048]{1,0:T(8,128)(2,1)} %param.17, s32[]{:T(128)S(6)} %select_n.131, bf16[256,1024]{0,1:T(8,128)(2,1)S(1)} %fusion.67, s32[]{:T(128)S(6)} %select_n.132), kind=kOutput, calls=%fused_computation.27 | convolution fusion | flops 536870912 | bytes 5505032 | tf_op jit(solution)/shard_map/dot_general | solution.py:104
  20.9 0.2 slice_reduce_fusion
  21.7 1.4 scatter_custom_fusion
  23.2 0.9 collective-permute-done.1
  24.1 4.0 %multiply_reduce_fusion.2 = (f32[128]{0:T(128)S(1)}, f32[128,2048]{1,0:T(8,128)S(1)}) fusion(f32[128,2048]{1,0:T(8,128)S(1)} %collective-permute-done.1, bf16[2048,2048]{1,0:T(8,128)(2,1)} %param.17, s32[]{:T(128)S(6)} %select_n.131, bf16[256,1024]{0,1:T(8,128)(2,1)S(1)} %fusion.67, s32[]{:T(128)S(6)} %select_n.130), kind=kOutput, calls=%fused_computation.67 | convolution fusion | flops 538181504 | bytes 6554120 | tf_op jit(solution)/shard_map/dot_general | solution.py:104
  28.2 0.4 fusion.63
  28.6 0.3 copy-done.10
  29.0 2.5 %gather_fusion = bf16[512,2048]{1,0:T(8,128)(2,1)S(1)} fusion(bf16[128,2048]{1,0:T(8,128)(2,1)S(1)} %fusion.65, s32[1024]{0:T(1024)S(1)} %pad_clamp_fusion.1), kind=kCustom, calls=%fused_computation | custom fusion | bytes 4196352 | tf_op jit(solution)/shard_map/gather | solution.py:128
  31.5 0.2 broadcast_select_fusion
  31.7 1.2 fusion.116
  32.9 33.1 %all_to_all.20 = bf16[8,32,2048]{2,1,0:T(8,128)(2,1)S(1)} all-to-all(bf16[8,32,2048]{2,1,0:T(8,128)(2,1)S(1)} %get-tuple-element.7), channel_id=1, replica_groups={{0,4,8,12,16,20,24,28},{2,6,10,14,18,22,26,30},{1,5,9,13,17,21,25,29},{..., dimensions={0} | all-to-all | bytes 2097152 | tf_op jit(solution)/shard_map/all_to_all | solution.py:143
  66.0 3.7 %all-to-all-start.2 = ((bf16[8,32,2048]{2,1,0:T(8,128)(2,1)}), bf16[8,32,2048]{2,1,0:T(8,128)(2,1)S(1)}, u32[]{:S(2)}, u32[]{:S(2)}) async-start(bf16[8,32,2048]{2,1,0:T(8,128)(2,1)} %get-tuple-element.8), calls=%async_computation.2 | async-start | bytes 2097152 | tf_op jit(solution)/shard_map/all_to_all | solution.py:143
  69.7 0.6 collective-permute-start.2
  70.3 24.9 %all-to-all-done.2 = bf16[8,32,2048]{2,1,0:T(8,128)(2,1)S(1)} async-done(((bf16[8,32,2048]{2,1,0:T(8,128)(2,1)}), bf16[8,32,2048]{2,1,0:T(8,128)(2,1)S(1)}, u32[]{:S(2)}, u32[]{:S(2)}) %all-to-all-start.2) | async-done | bytes 1048608 | tf_op jit(solution)/shard_map/all_to_all | solution.py:143
  95.2 0.7 collective-permute-start.4
  95.9 6.4 %fusion.12 = f32[256,1792]{1,0:T(8,128)} fusion(bf16[256,2048]{1,0:T(8,128)(2,1)S(1)} %bitcast.108, bf16[1,2048,1792]{2,1,0:T(8,128)(2,1)} %all-gather.9.cloned.1.call-done), kind=kOutput, calls=%fused_computation.15 | convolution fusion | flops 1879048192 | bytes 10223616 | tf_op jit(solution)/shard_map/dot_general | solution.py:42
  102.4 11.3 %fusion.37 = bf16[256,2048]{1,0:T(8,128)(2,1)} fusion(bf16[1,1792,2048]{2,1,0:T(8,128)(2,1)} %all-gather.11.cloned.1.call-done, f32[256,1792]{1,0:T(8,128)} %fusion.12, bf16[256,2048]{1,0:T(8,128)(2,1)S(1)} %bitcast.109, bf16[1,2048,1792]{2,1,0:T(8,128)(2,1)} %all-gather.7.cloned.1.call-done), kind=kOutput, calls=%fused_computation.34 | convolution fusion | flops 3761373184 | bytes 18612224 | tf_op jit(solution)/shard_map/dot_general | solution.py:44
  113.7 1.3 collective-permute-start.3
  114.9 6.4 %collective-permute-done.4 = bf16[8,32,2048]{2,1,0:T(8,128)(2,1)} collective-permute-done((bf16[8,32,2048]{2,1,0:T(8,128)(2,1)S(1)}, bf16[8,32,2048]{2,1,0:T(8,128)(2,1)}, u32[]{:S(2)}, u32[]{:S(2)}) %collective-permute-start.4) | collective-permute-done | bytes 1048608 | tf_op jit(solution)/shard_map/ppermute | solution.py:157
  121.3 6.8 %fusion.8 = f32[256,1792]{1,0:T(8,128)} fusion(bf16[256,2048]{1,0:T(8,128)(2,1)} %bitcast.18, bf16[1,2048,1792]{2,1,0:T(8,128)(2,1)} %all-gather.9.cloned.1.call-done), kind=kOutput, calls=%fused_computation.11 | convolution fusion | flops 1879048192 | bytes 10223616 | tf_op jit(solution)/shard_map/dot_general | solution.py:42
  128.1 11.6 %fusion.43 = bf16[256,2048]{1,0:T(8,128)(2,1)} fusion(bf16[1,1792,2048]{2,1,0:T(8,128)(2,1)} %all-gather.11.cloned.1.call-done, f32[256,1792]{1,0:T(8,128)} %fusion.8, bf16[256,2048]{1,0:T(8,128)(2,1)} %bitcast.18, bf16[1,2048,1792]{2,1,0:T(8,128)(2,1)} %all-gather.7.cloned.1.call-done), kind=kOutput, calls=%fused_computation.36 | convolution fusion | flops 3761373184 | bytes 18612224 | tf_op jit(solution)/shard_map/dot_general | solution.py:44
  139.7 0.7 collective-permute-start.5
  140.5 6.7 %fusion.22 = f32[256,1792]{1,0:T(8,128)} fusion(bf16[256,2048]{1,0:T(8,128)(2,1)S(1)} %bitcast.102, bf16[1,2048,1792]{2,1,0:T(8,128)(2,1)} %all-gather.7.cloned.1.call-done), kind=kOutput, calls=%fused_computation.25 | convolution fusion | flops 1879048192 | bytes 10223616 | tf_op jit(solution)/shard_map/dot_general | solution.py:41
  147.1 10.5 %fusion.34 = bf16[256,2048]{1,0:T(8,128)(2,1)S(1)} fusion(bf16[1,1792,2048]{2,1,0:T(8,128)(2,1)} %all-gather.11.cloned.1.call-done, bf16[256,2048]{1,0:T(8,128)(2,1)} %bitcast.103, bf16[1,2048,1792]{2,1,0:T(8,128)(2,1)} %all-gather.9.cloned.1.call-done, f32[256,1792]{1,0:T(8,128)} %fusion.22), kind=kOutput, calls=%fused_computation.33 | convolution fusion | flops 3761373184 | bytes 18612224 | tf_op jit(solution)/shard_map/dot_general | solution.py:44
  157.7 1.4 fusion.62
  159.1 3.8 %all-to-all-start.1 = ((bf16[8,32,2048]{2,1,0:T(8,128)(2,1)}), bf16[8,32,2048]{2,1,0:T(8,128)(2,1)S(1)}, u32[]{:S(2)}, u32[]{:S(2)}) async-start(bf16[8,32,2048]{2,1,0:T(8,128)(2,1)} %fusion.62), calls=%async_computation.1 | async-start | bytes 2097152 | tf_op jit(solution)/shard_map/all_to_all | solution.py:143
  162.8 6.4 %fusion.18 = f32[256,1792]{1,0:T(8,128)} fusion(bf16[256,2048]{1,0:T(8,128)(2,1)S(1)} %bitcast.101, bf16[1,2048,1792]{2,1,0:T(8,128)(2,1)} %all-gather.7.cloned.1.call-done), kind=kOutput, calls=%fused_computation.21 | convolution fusion | flops 1879048192 | bytes 10223616 | tf_op jit(solution)/shard_map/dot_general | solution.py:41
  169.2 10.5 %fusion.40 = bf16[256,2048]{1,0:T(8,128)(2,1)S(1)} fusion(bf16[1,1792,2048]{2,1,0:T(8,128)(2,1)} %all-gather.11.cloned.1.call-done, bf16[256,2048]{1,0:T(8,128)(2,1)} %bitcast.100, bf16[1,2048,1792]{2,1,0:T(8,128)(2,1)} %all-gather.9.cloned.1.call-done, f32[256,1792]{1,0:T(8,128)} %fusion.18), kind=kOutput, calls=%fused_computation.35 | convolution fusion | flops 3761373184 | bytes 18612224 | tf_op jit(solution)/shard_map/dot_general | solution.py:44
  179.8 1.4 fusion.61
  181.2 5.7 %all-to-all-done.1 = bf16[8,32,2048]{2,1,0:T(8,128)(2,1)S(1)} async-done(((bf16[8,32,2048]{2,1,0:T(8,128)(2,1)}), bf16[8,32,2048]{2,1,0:T(8,128)(2,1)S(1)}, u32[]{:S(2)}, u32[]{:S(2)}) %all-to-all-start.1) | async-done | bytes 1048608 | tf_op jit(solution)/shard_map/all_to_all | solution.py:143
  186.9 4.5 %all-to-all-start.3 = ((bf16[8,32,2048]{2,1,0:T(8,128)(2,1)}), bf16[8,32,2048]{2,1,0:T(8,128)(2,1)}, u32[]{:S(2)}, u32[]{:S(2)}) async-start(bf16[8,32,2048]{2,1,0:T(8,128)(2,1)} %fusion.61), calls=%async_computation.3 | async-start | bytes 2097152 | tf_op jit(solution)/shard_map/all_to_all | solution.py:143
  191.6 24.7 %all-to-all-done.3 = bf16[8,32,2048]{2,1,0:T(8,128)(2,1)} async-done(((bf16[8,32,2048]{2,1,0:T(8,128)(2,1)}), bf16[8,32,2048]{2,1,0:T(8,128)(2,1)}, u32[]{:S(2)}, u32[]{:S(2)}) %all-to-all-start.3) | async-done | bytes 1048608 | tf_op jit(solution)/shard_map/all_to_all | solution.py:143
  216.3 1.4 pad_maximum_fusion
  217.6 1.4 gather_fusion.1
  219.0 1.3 reshape.150
  220.4 3.2 %multiply_reduce_fusion = f32[128,2048]{1,0:T(8,128)S(1)} fusion(f32[128,2,2048]{2,1,0:T(2,128)S(1)} %reshape.150, f32[128,2]{1,0:T(8,128)S(1)} %copy.19), kind=kLoop, calls=%fused_computation.47 | loop fusion | flops 786432 | bytes 3146752 | tf_op jit(solution)/shard_map/reduce_sum | solution.py:166
  223.7 1.0 fusion.66
  (69 shorter events, 2.4 us)
Async XLA Ops:
  6.5 9.7 %copy-start = (bf16[2,512,512]{2,1,0:T(8,128)(2,1)S(1)}, bf16[2,512,512]{2,1,0:T(8,128)(2,1)}, u32[]{:S(2)}) copy-start(bf16[2,512,512]{2,1,0:T(8,128)(2,1)} %param.15) | copy-start | bytes 3145732
  6.5 89.4 %all-gather.9.cloned.1.call-start = ((), (), s32[]{:S(2)}) async-start(), calls=%async_computation.5 | async-start | bytes 11010048 | tf_op jit(solution)/shard_map/all_gather | solution.py:135
  7.3 1.0 copy-start.4
  7.3 95.1 %all-gather.11.cloned.1.call-start = ((), (), s32[]{:S(2)}) async-start(), calls=%async_computation.6 | async-start | bytes 11010048 | tf_op jit(solution)/shard_map/all_gather | solution.py:137
  8.0 5.2 %copy-start.13 = (s32[128,2]{0,1:T(2,128)S(1)}, s32[128,2]{0,1:T(2,128)}, u32[]{:S(2)}) copy-start(s32[128,2]{0,1:T(2,128)} %param.21) | copy-start | bytes 3076
  8.0 94.3 %all-gather.7.cloned.1.call-start = ((), (), s32[]{:S(2)}) async-start(), calls=%async_computation.4 | async-start | bytes 11010048 | tf_op jit(solution)/shard_map/all_gather | solution.py:134
  8.3 6.4 %collective-permute-start = (bf16[16,1024]{1,0:T(8,128)(2,1)S(1)}, bf16[16,1024]{1,0:T(8,128)(2,1)S(1)}, u32[]{:S(2)}, u32[]{:S(2)}) collective-permute-start(bf16[16,1024]{1,0:T(8,128)(2,1)S(1)} %slice.81), channel_id=1, source_target_pairs={{0,2},{2,4},{4,6},{6,8},{8,10},{10,12},{12,14},{14,16},{16,18},{18... | collective-permute-start | bytes 98312 | tf_op jit(solution)/shard_map/ppermute | solution.py:18
  16.2 0.8 copy-start.12
  20.8 3.2 %collective-permute-start.1 = (f32[128,2048]{1,0:T(8,128)S(1)}, f32[128,2048]{1,0:T(8,128)S(1)}, u32[]{:S(2)}, u32[]{:S(2)}) collective-permute-start(f32[128,2048]{1,0:T(8,128)S(1)} %fusion.24), channel_id=1, source_target_pairs={{0,1},{1,0},{2,3},{3,2},{4,5},{5,4},{6,7},{7,6},{8,9},{9,8},{10,11... | collective-permute-start | bytes 3145736 | tf_op jit(solution)/shard_map/ppermute | solution.py:110
  23.2 5.0 %copy-start.8 = (bf16[128,2048]{1,0:T(8,128)(2,1)S(1)}, bf16[128,2048]{1,0:T(8,128)(2,1)}, u32[]{:S(2)}) copy-start(bf16[128,2048]{1,0:T(8,128)(2,1)} %param.13) | copy-start | bytes 1572868
  23.2 5.0 %copy-start.9 = (f32[2048]{0:T(1024)S(1)}, f32[2048]{0:T(1024)}, u32[]{:S(2)}) copy-start(f32[2048]{0:T(1024)} %param.18) | copy-start | bytes 24580
  28.1 0.7 copy-start.10
  28.5 3.0 %copy-start.2 = (bf16[128,2048]{1,0:T(8,128)(2,1)}, bf16[128,2048]{1,0:T(8,128)(2,1)S(1)}, u32[]{:S(2)}) copy-start(bf16[128,2048]{1,0:T(8,128)(2,1)S(1)} %get-tuple-element.6) | copy-start | bytes 1572868
  66.0 74.5 %copy-start.7 = (bf16[8,32,2048]{2,1,0:T(8,128)(2,1)}, bf16[8,32,2048]{2,1,0:T(8,128)(2,1)S(1)}, u32[]{:S(2)}) copy-start(bf16[8,32,2048]{2,1,0:T(8,128)(2,1)S(1)} %all_to_all.20) | copy-start | bytes 3145732
  66.0 29.2 %all-to-all-start.2 = ((bf16[8,32,2048]{2,1,0:T(8,128)(2,1)}), bf16[8,32,2048]{2,1,0:T(8,128)(2,1)S(1)}, u32[]{:S(2)}, u32[]{:S(2)}) async-start(bf16[8,32,2048]{2,1,0:T(8,128)(2,1)} %get-tuple-element.8), calls=%async_computation.2 | async-start | bytes 2097152 | tf_op jit(solution)/shard_map/all_to_all | solution.py:143
  69.7 26.2 %collective-permute-start.2 = (bf16[8,32,2048]{2,1,0:T(8,128)(2,1)S(1)}, bf16[8,32,2048]{2,1,0:T(8,128)(2,1)S(1)}, u32[]{:S(2)}, u32[]{:S(2)}) collective-permute-start(bf16[8,32,2048]{2,1,0:T(8,128)(2,1)S(1)} %all_to_all.20), channel_id=1, source_target_pairs={{0,2},{2,0},{4,6},{6,4},{8,10},{10,8},{12,14},{14,12},{16,18},{18,... | collective-permute-start | bytes 3145736 | tf_op jit(solution)/shard_map/ppermute | solution.py:157
  95.2 7.2 %copy-start.5 = (bf16[8,32,2048]{2,1,0:T(8,128)(2,1)}, bf16[8,32,2048]{2,1,0:T(8,128)(2,1)S(1)}, u32[]{:S(2)}) copy-start(bf16[8,32,2048]{2,1,0:T(8,128)(2,1)S(1)} %all-to-all-done.2) | copy-start | bytes 3145732
  95.2 26.1 %collective-permute-start.4 = (bf16[8,32,2048]{2,1,0:T(8,128)(2,1)S(1)}, bf16[8,32,2048]{2,1,0:T(8,128)(2,1)}, u32[]{:S(2)}, u32[]{:S(2)}) collective-permute-start(bf16[8,32,2048]{2,1,0:T(8,128)(2,1)S(1)} %all-to-all-done.2), channel_id=1, source_target_pairs={{0,2},{2,0},{4,6},{6,4},{8,10},{10,8},{12,14},{14,12},{16,18},{18,... | collective-permute-start | bytes 3145736 | tf_op jit(solution)/shard_map/ppermute | solution.py:157
  113.7 44.0 %collective-permute-start.3 = (bf16[8,32,2048]{2,1,0:T(8,128)(2,1)}, bf16[8,32,2048]{2,1,0:T(8,128)(2,1)S(1)}, u32[]{:S(2)}, u32[]{:S(2)}) collective-permute-start(bf16[8,32,2048]{2,1,0:T(8,128)(2,1)} %bitcast.110), channel_id=1, source_target_pairs={{0,2},{2,0},{4,6},{6,4},{8,10},{10,8},{12,14},{14,12},{16,18},{18,... | collective-permute-start | bytes 3145736 | tf_op jit(solution)/shard_map/ppermute | solution.py:160
  139.7 40.1 %collective-permute-start.5 = (bf16[8,32,2048]{2,1,0:T(8,128)(2,1)}, bf16[8,32,2048]{2,1,0:T(8,128)(2,1)S(1)}, u32[]{:S(2)}, u32[]{:S(2)}) collective-permute-start(bf16[8,32,2048]{2,1,0:T(8,128)(2,1)} %bitcast.107), channel_id=1, source_target_pairs={{0,2},{2,0},{4,6},{6,4},{8,10},{10,8},{12,14},{14,12},{16,18},{18,... | collective-permute-start | bytes 3145736 | tf_op jit(solution)/shard_map/ppermute | solution.py:160
  159.1 3.8 %copy-start.6 = (bf16[8,32,2048]{2,1,0:T(8,128)(2,1)S(1)}, bf16[8,32,2048]{2,1,0:T(8,128)(2,1)}, u32[]{:S(2)}) copy-start(bf16[8,32,2048]{2,1,0:T(8,128)(2,1)} %copy-done.5) | copy-start | bytes 3145732
  159.1 27.9 %all-to-all-start.1 = ((bf16[8,32,2048]{2,1,0:T(8,128)(2,1)}), bf16[8,32,2048]{2,1,0:T(8,128)(2,1)S(1)}, u32[]{:S(2)}, u32[]{:S(2)}) async-start(bf16[8,32,2048]{2,1,0:T(8,128)(2,1)} %fusion.62), calls=%async_computation.1 | async-start | bytes 2097152 | tf_op jit(solution)/shard_map/all_to_all | solution.py:143
  179.8 11.6 %copy-start.14 = (f32[128,2]{0,1:T(2,128)S(1)}, f32[128,2]{0,1:T(2,128)}, u32[]{:S(2)}) copy-start(f32[128,2]{0,1:T(2,128)} %param.22) | copy-start | bytes 3076
  186.9 29.3 %all-to-all-start.3 = ((bf16[8,32,2048]{2,1,0:T(8,128)(2,1)}), bf16[8,32,2048]{2,1,0:T(8,128)(2,1)}, u32[]{:S(2)}, u32[]{:S(2)}) async-start(bf16[8,32,2048]{2,1,0:T(8,128)(2,1)} %fusion.61), calls=%async_computation.3 | async-start | bytes 2097152 | tf_op jit(solution)/shard_map/all_to_all | solution.py:143
  220.3 3.4 %copy-start.3 = (bf16[128,2048]{1,0:T(8,128)(2,1)S(1)}, bf16[128,2048]{1,0:T(8,128)(2,1)}, u32[]{:S(2)}) copy-start(bf16[128,2048]{1,0:T(8,128)(2,1)} %copy-done.2) | copy-start | bytes 1572868
  220.4 3.4 %copy-start.11 = (f32[2048]{0:T(1024)S(1)}, f32[2048]{0:T(1024)}, u32[]{:S(2)}) copy-start(f32[2048]{0:T(1024)} %param.20) | copy-start | bytes 24580
  220.4 4.4 %copy-start.1 = (bf16[2,512,512]{2,1,0:T(8,128)(2,1)S(1)}, bf16[2,512,512]{2,1,0:T(8,128)(2,1)}, u32[]{:S(2)}) copy-start(bf16[2,512,512]{2,1,0:T(8,128)(2,1)} %param.15) | copy-start | bytes 3145732
Sparse Core Ops, SparseCore 0:
  8.9 20.9 all-gather.8
  31.4 19.5 all-gather.10
  52.5 19.3 all-gather.6
